TPU v7x, 32 devices: a whole 2x2x4 slice. The times are simulated.
32 devices in a mesh: ep: 8 (over z, core), tp: 4 (over y, x).
Axes of the slice: x: 2, y: 2, z: 4, core: 2. Of those that a mesh axis runs over, the one named last changes fastest.
Arguments:
- tokens: bfloat16 [1536, 4096], P('ep'), may hold values from -6 to 6
- expert_ids: int32 [1536, 2], P('ep'), may hold values from 0 to 7, all different within a row; in each aligned block of 192 rows (0 to 191, 192 to 383, ...) at most 60 rows name the same one
- route_weight: float32 [1536, 2], P('ep'), may hold values from 0.1 to 1
- norm_gain: float32 [4096], replicated, may hold values from 0.1 to 1.9
- gate_weight: bfloat16 [8, 4096, 4096], P('ep', None, 'tp'), may hold values from -0.28125 to 0.28125
- up_weight: bfloat16 [8, 4096, 4096], P('ep', None, 'tp'), may hold values from -0.28125 to 0.28125
- down_weight: bfloat16 [8, 4096, 4096], P('ep', None, 'tp'), may hold values from -0.028076172 to 0.028076172
Outputs:
- mixed: bfloat16 [1536, 4096], P('ep', 'tp')
Inputs may be any that keep to these rules, and one draw needn't show every extreme that they name: `expert_ids`: each row names 2 different experts. In each aligned block of 192 rows (the tokens of one index of ep) no expert is named by more than 60 rows, and in some block some expert is named by exactly 60 rows.
All inputs are finite; a program needn't handle non-finite values.
Results may differ from a plain program's by a relative error of at most 0.007.
Values may be sent and summed in bfloat16 or wider, within the bound.
A program may use at most 64 MiB of HBM per device.

v0:
```python
import jax
import jax.numpy as jnp
from jax import lax
from jax.sharding import PartitionSpec as P

EPS = 1e-06
LIMIT = 7.0
ALPHA = 1.702


def rms_norm(tokens, norm_gain):
    values = tokens.astype(jnp.float32)
    scale = lax.rsqrt(jnp.mean(values * values, axis=-1, keepdims=True) + EPS)
    return (values * scale * norm_gain).astype(jnp.bfloat16)


def clamped_unit(gate_pre, up_pre):
    gate = jnp.minimum(gate_pre, LIMIT)
    up_part = jnp.clip(up_pre, -LIMIT, LIMIT)
    return ((up_part + 1.0) * gate * jax.nn.sigmoid(ALPHA * gate)).astype(jnp.bfloat16)


def slot_numbers(id_blocks, experts, capacity):
    onehot = (id_blocks[:, :, None] == jnp.arange(experts, dtype=jnp.int32)[None, None, :]).astype(
        jnp.int32
    )
    before = jnp.cumsum(onehot, axis=1) - onehot
    position = jnp.sum(before * onehot, axis=2)
    return id_blocks * capacity + position


def project_down(hidden, down_weight):
    result = jnp.einsum(
        "sejf,efd->sejd",
        lax.all_gather(hidden, "tp", axis=3, tiled=True),
        down_weight,
        preferred_element_type=jnp.float32,
    )
    return result.astype(jnp.bfloat16)


def on_device(tokens, expert_ids, route_weight, norm_gain, gate_weight, up_weight, down_weight):
    n_ep = lax.axis_size("ep")
    n_tp = lax.axis_size("tp")
    tok_rows, width = tokens.shape
    top = expert_ids.shape[1]
    local_experts = gate_weight.shape[0]
    experts = local_experts * n_ep
    capacity = 5 * tok_rows * top // (4 * experts)
    cols = width // n_tp
    normed = rms_norm(tokens, norm_gain)
    dest = slot_numbers(expert_ids.reshape(1, tok_rows * top), experts, capacity).reshape(-1)
    slot_range = jnp.arange(experts * capacity, dtype=jnp.int32)
    match = slot_range[:, None] == dest[None, :]
    pick = jnp.any(match.reshape(experts * capacity, tok_rows, top), axis=2).astype(jnp.bfloat16)
    own = lax.dynamic_slice_in_dim(normed, lax.axis_index("tp") * cols, cols, 1)
    buffer = jnp.dot(pick, own, preferred_element_type=jnp.float32).astype(jnp.bfloat16)
    buffer = buffer.reshape(n_ep, local_experts, capacity, cols)
    arrived = lax.all_to_all(buffer, "ep", split_axis=0, concat_axis=0, tiled=True)
    piece = lax.all_gather(arrived, "tp", axis=3, tiled=True)
    gate_part = jnp.einsum("sejd,edf->sejf", piece, gate_weight, preferred_element_type=jnp.float32)
    up_part = jnp.einsum("sejd,edf->sejf", piece, up_weight, preferred_element_type=jnp.float32)
    hidden = clamped_unit(gate_part, up_part)
    result = project_down(hidden, down_weight)
    back = lax.all_to_all(result, "ep", split_axis=0, concat_axis=0, tiled=True).reshape(
        experts * capacity, cols
    )
    chosen = jnp.transpose(match).astype(jnp.bfloat16)
    per_copy = jnp.dot(chosen, back, preferred_element_type=jnp.float32).reshape(
        tok_rows, top, cols
    )
    mixed = jnp.sum(per_copy * route_weight[:, :, None], axis=1)
    return mixed.astype(jnp.bfloat16)


def solution(mesh):
    placed = (
        P("ep", None),
        P("ep", None),
        P("ep", None),
        P(),
        P("ep", None, "tp"),
        P("ep", None, "tp"),
        P("ep", None, "tp"),
    )
    return jax.shard_map(
        on_device, mesh=mesh, in_specs=placed, out_specs=P("ep", "tp"), check_vma=False
    )
```

profile of v0, /device:TPU:0, one launch (start us, length us, event | category | flops | bytes accessed | tf_op | source)
XLA Modules:
  0.0 220.5 jit_solution(3522461065963199480)
XLA Ops:
  6.5 0.0 copy-start
  6.5 0.0 all-gather.3.cloned.1.call-start
  6.5 0.0 copy-start.1
  6.5 3.5 %convert_element_type.41 = f32[192,4096]{1,0:T(8,128)} convert(bf16[192,4096]{1,0:T(8,128)(2,1)} %param.7) | non-fusion elementwise | flops 786432 | bytes 4718592 | tf_op jit(solution)/shard_map/convert_element_type | solution.py:12
  10.1 0.0 copy-done
  10.1 0.4 multiply_reduce_fusion
  10.5 0.0 copy-done.1
  10.5 0.1 copy.28
  10.6 0.1 reshape.211
  10.8 0.9 reduce-window.6
  11.6 0.2 slice_reduce_fusion
  11.9 0.1 fusion.36
  12.0 0.1 reduce_sum.30
  12.1 0.1 copy.29
  12.2 0.2 fusion.30
  12.4 0.7 dynamic-slice
  13.1 1.6 convolution_convert_fusion
  14.8 0.2 reshape.217
  14.9 32.8 %all_to_all.10 = bf16[8,1,60,1024]{3,2,1,0:T(8,128)(2,1)} all-to-all(bf16[8,1,60,1024]{3,2,1,0:T(8,128)(2,1)S(1)} %bitcast.73), channel_id=1, replica_groups=mesh['ep'=8,'tp'=4] {'ep'}, dimensions={0} | all-to-all | bytes 1966080 | tf_op jit(solution)/shard_map/all_to_all | solution.py:59
  47.8 0.0 all-gather.3.cloned.1.call-update
  47.8 0.0 all-gather.5.cloned.1.call-start
  47.8 51.6 %all-gather.3.cloned.1.call-done = bf16[8,1,60,4096]{3,2,0,1:T(8,128)(2,1)} async-done(((bf16[8,1,60,1024]{3,2,0,1:T(8,128)(2,1)}), bf16[8,1,60,4096]{3,2,0,1:T(8,128)(2,1)}) %all-gather.3.cloned.1.call-update) | async-done | bytes 3932176 | tf_op jit(solution)/shard_map/all_gather | solution.py:60
  99.4 0.0 copy-start.2
  99.4 9.1 %fusion.2 = f32[8,60,1024]{2,1,0:T(8,128)S(1)} fusion(bf16[1,4096,1024]{2,1,0:T(8,128)(2,1)} %param.11, bf16[8,1,60,4096]{3,2,0,1:T(8,128)(2,1)} %all-gather.3.cloned.1.call-done), kind=kOutput, calls=%fused_computation.2 | convolution fusion | flops 4026531840 | bytes 14286848 | tf_op jit(solution)/shard_map/sejd,edf->sejf/dot_general | solution.py:61
  108.6 0.0 copy-done.2
  108.6 9.4 %fusion.23 = bf16[8,1,60,1024]{3,2,0,1:T(8,128)(2,1)} fusion(f32[8,60,1024]{2,1,0:T(8,128)S(1)} %fusion.2, bf16[1,4096,1024]{2,1,0:T(8,128)(2,1)} %param.12, bf16[8,1,60,4096]{3,2,0,1:T(8,128)(2,1)S(1)} %copy-done.2), kind=kOutput, calls=%fused_computation.15 | convolution fusion | flops 4031447040 | bytes 15269888 | tf_op jit(solution)/shard_map/sejd,edf->sejf/dot_general | solution.py:62
  118.0 0.0 all-gather.5.cloned.1.call-update
  118.0 52.7 %all-gather.5.cloned.1.call-done = bf16[8,1,60,4096]{3,2,0,1:T(8,128)(2,1)} async-done(((bf16[8,1,60,1024]{3,2,0,1:T(8,128)(2,1)}), bf16[8,1,60,4096]{3,2,0,1:T(8,128)(2,1)}) %all-gather.5.cloned.1.call-update) | async-done | bytes 3932176 | tf_op jit(solution)/shard_map/all_gather | solution.py:35
  170.7 10.1 %fusion.18 = bf16[8,1,60,1024]{3,2,1,0:T(8,128)(2,1)} fusion(bf16[1,4096,1024]{2,1,0:T(8,128)(2,1)} %param.13, bf16[8,1,60,4096]{3,2,0,1:T(8,128)(2,1)} %all-gather.5.cloned.1.call-done), kind=kOutput, calls=%fused_computation.14 | convolution fusion | flops 4027023360 | bytes 13303808 | tf_op jit(solution)/shard_map/sejf,efd->sejd/dot_general | solution.py:33
  180.8 0.0 copy-start.3
  180.8 4.7 %all-to-all-start.1 = ((bf16[8,1,60,1024]{3,2,1,0:T(8,128)(2,1)}), bf16[8,1,60,1024]{3,2,1,0:T(8,128)(2,1)S(1)}, u32[]{:S(2)}, u32[]{:S(2)}) async-start(bf16[8,1,60,1024]{3,2,1,0:T(8,128)(2,1)} %fusion.18), calls=%async_computation.1 | async-start | bytes 2097152 | tf_op jit(solution)/shard_map/all_to_all | solution.py:65
  185.6 0.2 iota_compare_fusion.1
  185.8 0.3 eq.60
  186.0 26.1 %all-to-all-done.1 = bf16[8,1,60,1024]{3,2,1,0:T(8,128)(2,1)S(1)} async-done(((bf16[8,1,60,1024]{3,2,1,0:T(8,128)(2,1)}), bf16[8,1,60,1024]{3,2,1,0:T(8,128)(2,1)S(1)}, u32[]{:S(2)}, u32[]{:S(2)}) %all-to-all-start.1) | async-done | bytes 983072 | tf_op jit(solution)/shard_map/all_to_all | solution.py:65
  212.1 0.2 reshape.235
  212.3 0.0 copy-done.3
  212.3 1.4 multiply_reduce_fusion.1
  (8 shorter events, 0.0 us)
Async XLA Ops:
  6.5 3.6 %copy-start = (bf16[192,4096]{1,0:T(8,128)(2,1)S(1)}, bf16[192,4096]{1,0:T(8,128)(2,1)}, u32[]{:S(2)}) copy-start(bf16[192,4096]{1,0:T(8,128)(2,1)} %param.7) | copy-start | bytes 4718596
  6.5 92.9 %all-gather.3.cloned.1.call-start = ((), (), s32[]{:S(2)}) async-start(), calls=%async_computation.2 | async-start | bytes 5242880 | tf_op jit(solution)/shard_map/all_gather | solution.py:60
  6.5 4.0 %copy-start.1 = (s32[192,2]{0,1:T(2,128)S(1)}, s32[192,2]{0,1:T(2,128)}, u32[]{:S(2)}) copy-start(s32[192,2]{0,1:T(2,128)} %param.8) | copy-start | bytes 4612
  47.8 122.9 %all-gather.5.cloned.1.call-start = ((), (), s32[]{:S(2)}) async-start(), calls=%async_computation.3 | async-start | bytes 5242880 | tf_op jit(solution)/shard_map/all_gather | solution.py:35
  99.4 9.1 %copy-start.2 = (bf16[8,1,60,4096]{3,2,0,1:T(8,128)(2,1)S(1)}, bf16[8,1,60,4096]{3,2,0,1:T(8,128)(2,1)}, u32[]{:S(2)}) copy-start(bf16[8,1,60,4096]{3,2,0,1:T(8,128)(2,1)} %all-gather.3.cloned.1.call-done) | copy-start | bytes 11796484
  180.8 31.5 %copy-start.3 = (f32[192,2]{0,1:T(2,128)S(1)}, f32[192,2]{0,1:T(2,128)}, u32[]{:S(2)}) copy-start(f32[192,2]{0,1:T(2,128)} %param.9) | copy-start | bytes 4612
  180.8 31.3 %all-to-all-start.1 = ((bf16[8,1,60,1024]{3,2,1,0:T(8,128)(2,1)}), bf16[8,1,60,1024]{3,2,1,0:T(8,128)(2,1)S(1)}, u32[]{:S(2)}, u32[]{:S(2)}) async-start(bf16[8,1,60,1024]{3,2,1,0:T(8,128)(2,1)} %fusion.18), calls=%async_computation.1 | async-start | bytes 2097152 | tf_op jit(solution)/shard_map/all_to_all | solution.py:65
Sparse Core Ops, SparseCore 0:
  47.9 51.4 all-gather.2
  118.1 52.5 all-gather.4
where the time goes:
time: 221 us
  waiting for transfers between devices  130 us (59%)
  blocking collectives  32.8 us (15%)
  matrix products  31.6 us (14%)
  between operations  13.5 us (6%)
  other arithmetic  5.26 us (2%)
  starting transfers between devices  4.78 us (2%)
    all_gather x1, waiting for transfers between devices, project_down(): lax.all_gather(hidden, 'tp', axis=3, tiled=True)  52.7 us
    all_gather x1, waiting for transfers between devices, on_device(): piece = lax.all_gather(arrived, 'tp', axis=3, tiled=True)  51.6 us
    all_to_all x1, blocking collectives, on_device(): lax.all_to_all(buffer, 'ep', split_axis=0, concat_axis=0, tiled=True)  32.8 us
    all_to_all x1, waiting for transfers between devices, on_device(): lax.all_to_all(result, 'ep', split_axis=0, concat_axis=0, tiled=True)  26.1 us
    dot_general x1, matrix products, project_down(): jnp.einsum('sejf,efd->sejd', lax.all_gather(hidden, 'tp', axis=3, tiled=T...  10.1 us
    dot_general x1, matrix products, on_device(): jnp.einsum('sejd,edf->sejf', piece, up_weight, preferred_element_type=jnp...  9.37 us
    dot_general x1, matrix products, on_device(): jnp.einsum('sejd,edf->sejf', piece, gate_weight, preferred_element_type=j...  9.13 us
    all_to_all x1, starting transfers between devices, on_device(): lax.all_to_all(result, 'ep', split_axis=0, concat_axis=0, tiled=True)  4.74 us
  transfers between devices with their start and end apart: 3, of which 3 were waited for; matrix products, arithmetic and copies ran while one was open for 0% of the time, Pallas kernels for 0%

commit v1 on v0

--- a/solution.py
+++ b/solution.py
@@ -6,6 +6,20 @@
 EPS = 1e-06
 LIMIT = 7.0
 ALPHA = 1.702
+
+
+def plan_layers_all(u, axis_key, pos_dim, shard_in):
+    aux = jax.lax.axis_size(axis_key)
+    left_arr = jax.lax.axis_index(axis_key)
+    ready, p_next, k_now = (aux, left_arr, u.shape[pos_dim])
+    ledger = [(dev_i, (dev_i + 1) % ready) for dev_i in range(ready)]
+    tmp, taken_in = (u, None)
+    for b in range(ready):
+        local_now = jax.lax.ppermute(tmp, axis_key, ledger) if b < ready - 1 else None
+        u1 = shard_in(tmp, (p_next - b) % ready * k_now)
+        taken_in = u1 if taken_in is None else taken_in + u1
+        tmp = local_now
+    return taken_in
 
 
 def rms_norm(tokens, norm_gain):
@@ -30,11 +44,16 @@
 
 
 def project_down(hidden, down_weight):
-    result = jnp.einsum(
-        "sejf,efd->sejd",
-        lax.all_gather(hidden, "tp", axis=3, tiled=True),
-        down_weight,
-        preferred_element_type=jnp.float32,
+    result = plan_layers_all(
+        hidden,
+        "tp",
+        3,
+        lambda own_block, start: jnp.einsum(
+            "sejf,efd->sejd",
+            own_block,
+            lax.dynamic_slice_in_dim(down_weight, start, own_block.shape[3], axis=1),
+            preferred_element_type=jnp.float32,
+        ),
     )
     return result.astype(jnp.bfloat16)
 

time: 221 us -> 229 us (1.036)
  waiting for transfers between devices: 130 us -> 138 us
    ppermute x0 -> x3, waiting for transfers between devices: none -> 60.5 us  [plan_layers_all(): jax.lax.ppermute(tmp, axis_key, ledger)]
    all_gather x1 -> x0, waiting for transfers between devices: 52.7 us -> none  [project_down(): lax.all_gather(hidden, 'tp', axis=3, tiled=True)]
    dot_general x1 -> x4, matrix products: 10.1 us -> 9.88 us  [project_down(): jnp.einsum('sejf,efd->sejd', own_block, lax.dynamic_slice_in_dim(down_wei...]
  transfers between devices with their start and end apart: 3 -> 5, of which waited for: 3 -> 5; matrix products, arithmetic and copies ran while one was open for 0% -> 3% of each run, Pallas kernels for 0% -> 0%
where the time goes in v1:
time: 229 us
  waiting for transfers between devices  138 us (60%)
  blocking collectives  32.8 us (14%)
  matrix products  30.2 us (13%)
  between operations  13.6 us (6%)
  starting transfers between devices  6.84 us (3%)
  local copies, waits for them, and re-layouts  3.75 us (2%)
  other arithmetic  3.58 us (2%)
    ppermute x3, waiting for transfers between devices, plan_layers_all(): jax.lax.ppermute(tmp, axis_key, ledger)  60.5 us
    all_gather x1, waiting for transfers between devices, on_device(): piece = lax.all_gather(arrived, 'tp', axis=3, tiled=True)  51.7 us
    all_to_all x1, blocking collectives, on_device(): lax.all_to_all(buffer, 'ep', split_axis=0, concat_axis=0, tiled=True)  32.8 us
    all_to_all x1, waiting for transfers between devices, on_device(): lax.all_to_all(result, 'ep', split_axis=0, concat_axis=0, tiled=True)  26.1 us
    dot_general x4, matrix products, project_down(): jnp.einsum('sejf,efd->sejd', own_block, lax.dynamic_slice_in_dim(down_wei...  9.88 us
    dot_general x1, matrix products, on_device(): jnp.einsum('sejd,edf->sejf', piece, gate_weight, preferred_element_type=j...  9.13 us
    dot_general x1, matrix products, on_device(): jnp.einsum('sejd,edf->sejf', piece, up_weight, preferred_element_type=jnp...  8.38 us
    all_to_all x1, starting transfers between devices, on_device(): lax.all_to_all(result, 'ep', split_axis=0, concat_axis=0, tiled=True)  4.75 us
  transfers between devices with their start and end apart: 5, of which 5 were waited for; matrix products, arithmetic and copies ran while one was open for 3% of the time, Pallas kernels for 0%

profile of v1, /device:TPU:0, one launch (start us, length us, event | category | flops | bytes accessed | tf_op | source)
XLA Modules:
  0.0 229.2 jit_solution(7607586606837907222)
XLA Ops:
  6.5 0.0 all-gather.2.cloned.1.call-start
  6.5 0.0 copy-start
  6.5 0.0 copy-start.1
  6.5 1.9 convert_element_type.33
  8.4 0.0 copy-done
  8.4 0.4 multiply_reduce_fusion
  8.8 0.0 copy-done.1
  8.8 0.1 copy.36
  9.0 0.1 reshape.235
  9.1 0.9 reduce-window.6
  10.0 0.2 slice_reduce_fusion
  10.2 0.1 fusion.41
  10.3 0.1 reduce_sum.30
  10.5 0.1 copy.37
  10.6 0.2 fusion.35
  10.7 0.7 dynamic-slice
  11.4 1.5 convolution_convert_fusion
  12.9 1.3 reshape.242
  14.3 32.8 %all_to_all.10 = bf16[8,1,60,1024]{3,2,1,0:T(8,128)(2,1)} all-to-all(bf16[8,1,60,1024]{3,2,1,0:T(8,128)(2,1)S(1)} %bitcast.81), channel_id=1, replica_groups=mesh['ep'=8,'tp'=4] {'ep'}, dimensions={0} | all-to-all | bytes 1966080 | tf_op jit(solution)/shard_map/all_to_all | solution.py:78
  47.1 0.0 all-gather.2.cloned.1.call-update
  47.1 51.7 %all-gather.2.cloned.1.call-done = bf16[8,1,60,4096]{3,2,0,1:T(8,128)(2,1)} async-done(((bf16[8,1,60,1024]{3,2,0,1:T(8,128)(2,1)}), bf16[8,1,60,4096]{3,2,0,1:T(8,128)(2,1)}) %all-gather.2.cloned.1.call-update) | async-done | bytes 3932176 | tf_op jit(solution)/shard_map/all_gather | solution.py:79
  98.8 0.0 copy-start.2
  98.8 9.1 %fusion = f32[8,60,1024]{2,1,0:T(8,128)S(1)} fusion(bf16[1,4096,1024]{2,1,0:T(8,128)(2,1)} %param.11, bf16[8,1,60,4096]{3,2,0,1:T(8,128)(2,1)} %all-gather.2.cloned.1.call-done), kind=kOutput, calls=%fused_computation | convolution fusion | flops 4026531840 | bytes 14286848 | tf_op jit(solution)/shard_map/sejd,edf->sejf/dot_general | solution.py:80
  107.9 0.0 copy-done.2
  107.9 8.4 %multiply_convert_fusion = bf16[8,60,1024]{2,1,0:T(8,128)(2,1)S(1)} fusion(f32[8,60,1024]{2,1,0:T(8,128)S(1)} %fusion, bf16[1,4096,1024]{2,1,0:T(8,128)(2,1)} %param.12, bf16[8,1,60,4096]{3,2,0,1:T(8,128)(2,1)S(1)} %copy-done.2), kind=kOutput, calls=%fused_computation.15 | convolution fusion | flops 4031447040 | bytes 15269888 | tf_op jit(solution)/shard_map/sejd,edf->sejf/dot_general | solution.py:81
  116.3 0.5 copy.40
  116.9 1.5 collective-permute-start
  118.4 22.8 %collective-permute-done = bf16[8,1,60,1024]{3,0,2,1:T(8,128)(2,1)S(1)} collective-permute-done((bf16[8,1,60,1024]{3,0,2,1:T(8,128)(2,1)S(1)}, bf16[8,1,60,1024]{3,0,2,1:T(8,128)(2,1)S(1)}, u32[]{:S(2)}, u32[]{:S(2)}) %collective-permute-start) | collective-permute-done | bytes 983072 | tf_op jit(solution)/shard_map/ppermute | solution.py:18
  141.1 0.6 collective-permute-start.1
  141.7 22.8 %collective-permute-done.1 = bf16[8,1,60,1024]{3,0,2,1:T(8,128)(2,1)S(1)} collective-permute-done((bf16[8,1,60,1024]{3,0,2,1:T(8,128)(2,1)S(1)}, bf16[8,1,60,1024]{3,0,2,1:T(8,128)(2,1)S(1)}, u32[]{:S(2)}, u32[]{:S(2)}) %collective-permute-start.1) | collective-permute-done | bytes 983072 | tf_op jit(solution)/shard_map/ppermute | solution.py:18
  164.5 0.0 collective-permute-start.2
  164.5 0.0 slice-start
  164.5 3.0 %fusion.12 = f32[1024,8,60]{0,2,1:T(8,128)S(1)} fusion(bf16[8,60,1024]{2,1,0:T(8,128)(2,1)S(1)} %multiply_convert_fusion, bf16[1,4096,1024]{2,1,0:T(8,128)(2,1)} %param.13, s32[]{:T(128)S(6)} %select_n.35), kind=kOutput, calls=%fused_computation.13 | convolution fusion | flops 1006632960 | bytes 5046276 | tf_op jit(solution)/shard_map/sejf,efd->sejd/dot_general | solution.py:51
  167.5 0.0 slice-start.1
  167.5 3.1 %fusion.10 = f32[1024,8,60]{0,2,1:T(8,128)S(1)} fusion(bf16[1,4096,1024]{2,1,0:T(8,128)(2,1)} %param.13, s32[]{:T(128)S(6)} %select_n.38, bf16[8,1,60,1024]{3,0,2,1:T(8,128)(2,1)S(1)} %collective-permute-done), kind=kOutput, calls=%fused_computation.11 | convolution fusion | flops 1006632960 | bytes 5046276 | tf_op jit(solution)/shard_map/sejf,efd->sejd/dot_general | solution.py:51
  170.6 0.0 slice-done
  170.6 0.0 slice-done.1
  170.7 1.4 fusion.8
  172.0 15.0 %collective-permute-done.2 = bf16[8,1,60,1024]{3,0,2,1:T(8,128)(2,1)S(1)} collective-permute-done((bf16[8,1,60,1024]{3,0,2,1:T(8,128)(2,1)S(1)}, bf16[8,1,60,1024]{3,0,2,1:T(8,128)(2,1)S(1)}, u32[]{:S(2)}, u32[]{:S(2)}) %collective-permute-start.2) | collective-permute-done | bytes 983072 | tf_op jit(solution)/shard_map/ppermute | solution.py:18
  187.0 2.4 %fusion.24 = bf16[8,1,60,1024]{3,2,1,0:T(8,128)(2,1)} fusion(bf16[1,4096,1024]{2,1,0:T(8,128)(2,1)S(1)} %bitcast.85, s32[]{:T(128)S(6)} %select_n.42, f32[1024,8,60]{0,2,1:T(8,128)S(1)} %fusion.8, f32[1024,8,60]{0,2,1:T(8,128)S(1)} %fusion.12, f32[1024,8,60]{0,2,1:T(8,128)S(1)} %fusion.10, bf16[8,1,60,1024]{3,0,2,1:T(8,128)(2,1)S(1)} %collective-permute-done.2), kind=kOutput, calls=%fused_computation.23 | convolution fusion | flops 1008599040 | bytes 10354692 | tf_op jit(solution)/shard_map/sejf,efd->sejd/dot_general | solution.py:51
  189.4 0.0 copy-start.3
  189.4 4.8 %all-to-all-start.1 = ((bf16[8,1,60,1024]{3,2,1,0:T(8,128)(2,1)}), bf16[8,1,60,1024]{3,2,1,0:T(8,128)(2,1)S(1)}, u32[]{:S(2)}, u32[]{:S(2)}) async-start(bf16[8,1,60,1024]{3,2,1,0:T(8,128)(2,1)} %fusion.24), calls=%async_computation.1 | async-start | bytes 2097152 | tf_op jit(solution)/shard_map/all_to_all | solution.py:84
  194.2 0.2 iota_compare_fusion.1
  194.4 0.3 eq.65
  194.6 26.1 %all-to-all-done.1 = bf16[8,1,60,1024]{3,2,1,0:T(8,128)(2,1)S(1)} async-done(((bf16[8,1,60,1024]{3,2,1,0:T(8,128)(2,1)}), bf16[8,1,60,1024]{3,2,1,0:T(8,128)(2,1)S(1)}, u32[]{:S(2)}, u32[]{:S(2)}) %all-to-all-start.1) | async-done | bytes 983072 | tf_op jit(solution)/shard_map/all_to_all | solution.py:84
  220.7 0.2 reshape.268
  220.9 0.0 copy-done.3
  220.9 1.4 multiply_reduce_fusion.1
  (9 shorter events, 0.0 us)
Async XLA Ops:
  6.5 92.2 %all-gather.2.cloned.1.call-start = ((), (), s32[]{:S(2)}) async-start(), calls=%async_computation.2 | async-start | bytes 5242880 | tf_op jit(solution)/shard_map/all_gather | solution.py:79
  6.5 1.9 copy-start
  6.5 2.3 copy-start.1
  98.8 9.1 %copy-start.2 = (bf16[8,1,60,4096]{3,2,0,1:T(8,128)(2,1)S(1)}, bf16[8,1,60,4096]{3,2,0,1:T(8,128)(2,1)}, u32[]{:S(2)}) copy-start(bf16[8,1,60,4096]{3,2,0,1:T(8,128)(2,1)} %all-gather.2.cloned.1.call-done) | copy-start | bytes 11796484
  116.9 24.3 %collective-permute-start = (bf16[8,1,60,1024]{3,0,2,1:T(8,128)(2,1)S(1)}, bf16[8,1,60,1024]{3,0,2,1:T(8,128)(2,1)S(1)}, u32[]{:S(2)}, u32[]{:S(2)}) collective-permute-start(bf16[8,1,60,1024]{3,0,2,1:T(8,128)(2,1)S(1)} %copy.40), channel_id=1, source_target_pairs={{0,1},{1,2},{2,3},{3,0},{4,5},{5,6},{6,7},{7,4},{8,9},{9,10},{10,1... | collective-permute-start | bytes 2949128 | tf_op jit(solution)/shard_map/ppermute | solution.py:18
  141.1 23.4 %collective-permute-start.1 = (bf16[8,1,60,1024]{3,0,2,1:T(8,128)(2,1)S(1)}, bf16[8,1,60,1024]{3,0,2,1:T(8,128)(2,1)S(1)}, u32[]{:S(2)}, u32[]{:S(2)}) collective-permute-start(bf16[8,1,60,1024]{3,0,2,1:T(8,128)(2,1)S(1)} %collective-permute-done), channel_id=1, source_target_pairs={{0,1},{1,2},{2,3},{3,0},{4,5},{5,6},{6,7},{7,4},{8,9},{9,10},{10,1... | collective-permute-start | bytes 2949128 | tf_op jit(solution)/shard_map/ppermute | solution.py:18
  164.5 22.5 %collective-permute-start.2 = (bf16[8,1,60,1024]{3,0,2,1:T(8,128)(2,1)S(1)}, bf16[8,1,60,1024]{3,0,2,1:T(8,128)(2,1)S(1)}, u32[]{:S(2)}, u32[]{:S(2)}) collective-permute-start(bf16[8,1,60,1024]{3,0,2,1:T(8,128)(2,1)S(1)} %collective-permute-done.1), channel_id=1, source_target_pairs={{0,1},{1,2},{2,3},{3,0},{4,5},{5,6},{6,7},{7,4},{8,9},{9,10},{10,1... | collective-permute-start | bytes 2949128 | tf_op jit(solution)/shard_map/ppermute | solution.py:18
  164.5 6.1 %slice-start = ((s8[8388608]{0:T(1024)(128)(4,1)}), s8[4194304]{0:T(1024)(128)(4,1)S(1)}, s32[]{:S(2)}) async-start(s8[8388608]{0:T(1024)(128)(4,1)} %bitcast.84), calls=%async_computation.3 | async-start | bytes 8388608
  167.5 3.1 %slice-start.1 = ((s8[8388608]{0:T(1024)(128)(4,1)}), s8[4194304]{0:T(1024)(128)(4,1)S(1)}, s32[]{:S(2)}) async-start(s8[8388608]{0:T(1024)(128)(4,1)} %bitcast.84), calls=%async_computation.4 | async-start | bytes 8388608
  189.4 31.5 %copy-start.3 = (f32[192,2]{0,1:T(2,128)S(1)}, f32[192,2]{0,1:T(2,128)}, u32[]{:S(2)}) copy-start(f32[192,2]{0,1:T(2,128)} %param.9) | copy-start | bytes 4612
  189.4 31.3 %all-to-all-start.1 = ((bf16[8,1,60,1024]{3,2,1,0:T(8,128)(2,1)}), bf16[8,1,60,1024]{3,2,1,0:T(8,128)(2,1)S(1)}, u32[]{:S(2)}, u32[]{:S(2)}) async-start(bf16[8,1,60,1024]{3,2,1,0:T(8,128)(2,1)} %fusion.24), calls=%async_computation.1 | async-start | bytes 2097152 | tf_op jit(solution)/shard_map/all_to_all | solution.py:84
Sparse Core Ops, SparseCore 0:
  47.2 51.4 all-gather.1
